TPU v7x, 256 devices: a whole 4x4x8 slice. The times are simulated.
256 devices in a mesh: ep: 64 (over z, x, core), tp: 4 (over y).
Axes of the slice: x: 4, y: 4, z: 8, core: 2. Of those that a mesh axis runs over, the one named last changes fastest.
Arguments:
- head_inputs_unfiltered: bfloat16 [8192, 4096], P('ep', 'tp'), may hold values from -6 to 6
- group_write_vectors: bfloat16 [8192, 512], P('ep', 'tp'), may hold values from -6 to 6
- group_read_vectors: bfloat16 [8192, 512], P('ep', 'tp'), may hold values from -6 to 6
- output_gate_inputs: bfloat16 [8192, 4096], P('ep', 'tp'), may hold values from -6 to 6
- step_preactivation: float32 [64, 8192], P('tp', 'ep'), may hold values from -3.2 to 3.6
- extra_decay_logs: float32 [64, 8192], P('tp', 'ep'), may hold values from -0.7 to 0
- head_decay_logs: float32 [64], P('tp'), may hold values from -16 to -2.7
- head_filter_taps: bfloat16 [4, 4096], P(None, 'tp'), may hold values from -3 to 3
- write_filter_taps: bfloat16 [4, 512], P(None, 'tp'), may hold values from -3 to 3
- read_filter_taps: bfloat16 [4, 512], P(None, 'tp'), may hold values from -3 to 3
- grouped_norm_gain: float32 [4096], P('tp'), may hold values from 0.1 to 1.9
- mixer_output_weight: bfloat16 [4096, 2048], P('tp'), may hold values from -0.09375 to 0.09375
- expert_input_rows: bfloat16 [32768, 2048], P(('ep', 'tp')), may hold values from -6 to 6
- expert_norm_gain: float32 [2048], replicated, may hold values from 0.1 to 1.9
- routes: int32 [32768, 2], P(('ep', 'tp')), may hold values from 0 to 63, all different within a row; in each aligned block of 128 rows (0 to 127, 128 to 255, ...) at most 6 rows name the same one
- router_chosen_scores: bfloat16 [32768, 2], P(('ep', 'tp')), may hold values from 0.049804688 to 1
- routed_gate_weight: bfloat16 [64, 2048, 1024], P('ep', None, 'tp'), may hold values from -0.125 to 0.125
- routed_up_weight: bfloat16 [64, 2048, 1024], P('ep', None, 'tp'), may hold values from -0.125 to 0.125
- routed_down_weight: bfloat16 [64, 1024, 2048], P('ep', 'tp'), may hold values from -0.1875 to 0.1875
- shared_gate_weight: bfloat16 [2048, 512], P(None, 'tp'), may hold values from -0.125 to 0.125
- shared_up_weight: bfloat16 [2048, 512], P(None, 'tp'), may hold values from -0.125 to 0.125
- shared_down_weight: bfloat16 [512, 2048], P('tp'), may hold values from -0.25 to 0.25
Outputs:
- mixer_result: bfloat16 [8192, 2048], P(('ep', 'tp'))
- moe_result: bfloat16 [32768, 2048], P(('ep', 'tp'))
Inputs may be any that keep to these rules, and one draw needn't show every extreme that they name: `routes`: within the 128 rows of one device no expert is named more than 6 times; a row names 2 different experts.
All inputs are finite; a program needn't handle non-finite values.
Results may differ from a plain program's by a relative error of at most 0.0095.
Values may be sent and summed in bfloat16 or wider, within the bound.
A program may use at most 128 MiB of HBM per device.

v0:
```python
import jax
import jax.numpy as jnp
from jax import lax
from jax.sharding import Mesh
from jax.sharding import PartitionSpec as P

HEAD_DIM = 64
STATE = 128
BLOCK = 64
EP = ("ep_0", "ep_1", "ep_2")
EP_TP = ("ep_0", "ep_1", "ep_2", "tp")


eps_norm = 1e-06
route_scale = 2.5
highest = lax.Precision.HIGHEST


def from_behind(value, axis, by):
    devices = lax.axis_size(axis)
    pairs = [(i, i + by) for i in range(devices) if 0 <= i + by < devices]
    return lax.ppermute(value, axis, pairs)


def filled_with(value, identity):
    return jax.tree.map(
        lambda part, zero: jnp.zeros_like(part) + jnp.asarray(zero, part.dtype), value, identity
    )


def entering_2(value, axes, combine, identity):
    before = start = filled_with(value, identity)
    running = value
    for axis in reversed(axes):
        devices, mine = (lax.axis_size(axis), lax.axis_index(axis))
        pieces = jax.tree.map(lambda part: lax.all_gather(part, axis), running)
        inside, running = (start, start)
        for k in range(devices):
            passed = k < mine
            running = combine(running, jax.tree.map(lambda part: part[k], pieces))
            inside = jax.tree.map(lambda new, old: jnp.where(passed, new, old), running, inside)
        before = combine(inside, before)
    return before


def split_up(value, dim, devices):
    before, after = (value.shape[:dim], value.shape[dim + 1 :])
    return jnp.moveaxis(value.reshape(*before, devices, -1, *after), dim, 0)


def summed_on_arrival(value, axis, dim):
    devices = lax.axis_size(axis)
    parts = lax.all_to_all(split_up(value, dim, devices), axis, 0, 0, tiled=True)
    return jnp.sum(parts.astype(jnp.float32), axis=0)


def conv_silu(values, weights):
    taps = weights.shape[0]
    length = values.shape[0] - taps + 1
    running_sum = jnp.zeros((length, values.shape[1]), jnp.float32)
    for offset in range(taps):
        running_sum = running_sum + weights[offset].astype(jnp.float32) * values[
            offset : offset + length
        ].astype(jnp.float32)
    return jax.nn.silu(running_sum)


def combine_states(earlier_part, later_part):
    return (
        earlier_part[0] + later_part[0],
        later_part[1] + jnp.exp(later_part[0])[..., None, None] * earlier_part[1],
    )


def mixer_rows(
    head_inputs_unfiltered,
    group_write_vectors,
    group_read_vectors,
    output_gate_inputs,
    step_preactivation,
    extra_decay_logs,
    head_decay_logs,
    head_filter_taps,
    write_filter_taps,
    read_filter_taps,
    grouped_norm_gain,
):
    row_total = head_inputs_unfiltered.shape[0]
    taps = head_filter_taps.shape[0]
    head_chans = head_inputs_unfiltered.shape[1]
    write_chans = group_write_vectors.shape[1]
    tail_rows = jnp.concatenate(
        [
            head_inputs_unfiltered[row_total - taps + 1 :],
            group_write_vectors[row_total - taps + 1 :],
            group_read_vectors[row_total - taps + 1 :],
        ],
        axis=1,
    )
    earlier = from_behind(tail_rows, EP, 1)
    padded_heads = jnp.concatenate([earlier[:, :head_chans], head_inputs_unfiltered], axis=0)
    padded_write = jnp.concatenate(
        [earlier[:, head_chans : head_chans + write_chans], group_write_vectors], axis=0
    )
    padded_read = jnp.concatenate(
        [earlier[:, head_chans + write_chans :], group_read_vectors], axis=0
    )
    heads_local = step_preactivation.shape[0]
    groups_local = write_chans // STATE
    per_group = heads_local // groups_local
    block_count = row_total // BLOCK
    head_values = conv_silu(padded_heads, head_filter_taps).reshape(
        block_count, BLOCK, groups_local, per_group, HEAD_DIM
    )
    write_values = conv_silu(padded_write, write_filter_taps).reshape(
        block_count, BLOCK, groups_local, STATE
    )
    read_values = conv_silu(padded_read, read_filter_taps).reshape(
        block_count, BLOCK, groups_local, STATE
    )
    step_length_value = jax.nn.softplus(step_preactivation)
    decay_rate_logs = -jnp.exp(head_decay_logs)[:, None] * step_length_value + extra_decay_logs
    step_blocks = step_length_value.reshape(groups_local, per_group, block_count, BLOCK)
    cumulative = jnp.cumsum(
        decay_rate_logs.reshape(groups_local, per_group, block_count, BLOCK), axis=3
    )
    weighted = head_values * jnp.transpose(step_blocks, (2, 3, 0, 1))[..., None]
    lower_mask = jnp.tril(jnp.ones((BLOCK, BLOCK), bool))
    gap_logs = cumulative[..., :, None] - cumulative[..., None, :]
    within = jnp.exp(jnp.where(lower_mask, gap_logs, -jnp.inf))
    affinity = jnp.einsum("blgn,bsgn->gbls", read_values, write_values, precision=highest)
    local_part = jnp.einsum(
        "gebls,bsgep->blgep", affinity[:, None] * within, weighted, precision=highest
    )
    to_end = jnp.exp(cumulative[..., -1:] - cumulative)
    block_states = jnp.einsum(
        "bsgn,bsgep,gebs->bgepn", write_values, weighted, to_end, precision=highest
    )
    block_decay = cumulative[..., -1]
    running = jnp.cumsum(block_decay, axis=2)
    entering = running - block_decay
    earlier_blocks = jnp.tril(jnp.ones((block_count, block_count), bool), -1)
    block_ratio = entering[..., :, None] - running[..., None, :]
    carry_weights = jnp.exp(jnp.where(earlier_blocks, block_ratio, -jnp.inf))
    inside = jnp.einsum("gebc,cgepn->bgepn", carry_weights, block_states, precision=highest)
    device_decay = running[..., -1]
    device_state = jnp.einsum(
        "gec,cgepn->gepn",
        jnp.exp(device_decay[..., None] - running),
        block_states,
        precision=highest,
    )
    scanned_pair = entering_2(
        (device_decay, device_state),
        EP,
        combine_states,
        (jnp.zeros_like(device_decay), jnp.zeros_like(device_state)),
    )
    incoming = scanned_pair[1]
    states_in = (
        inside + jnp.exp(jnp.transpose(entering, (2, 0, 1)))[..., None, None] * incoming[None]
    )
    carried_part = (
        jnp.einsum("blgn,bgepn->blgep", read_values, states_in, precision=highest)
        * jnp.transpose(jnp.exp(cumulative), (2, 3, 0, 1))[..., None]
    )
    scan_out = (local_part + carried_part).reshape(row_total, groups_local, per_group * HEAD_DIM)
    gate_values = jax.nn.silu(output_gate_inputs.astype(jnp.float32)).reshape(
        row_total, groups_local, per_group * HEAD_DIM
    )
    gated_rows = scan_out * gate_values
    gated_rows = gated_rows * lax.rsqrt(
        jnp.mean(gated_rows * gated_rows, axis=-1, keepdims=True) + eps_norm
    )
    return (gated_rows.reshape(row_total, head_chans) * grouped_norm_gain).astype(jnp.bfloat16)


def local(
    head_inputs_unfiltered,
    group_write_vectors,
    group_read_vectors,
    output_gate_inputs,
    step_preactivation,
    extra_decay_logs,
    head_decay_logs,
    head_filter_taps,
    write_filter_taps,
    read_filter_taps,
    grouped_norm_gain,
    mixer_output_weight,
    expert_input_rows,
    expert_norm_gain,
    routes,
    router_chosen_scores,
    routed_gate_weight,
    routed_up_weight,
    routed_down_weight,
    shared_gate_weight,
    shared_up_weight,
    shared_down_weight,
):
    mixer_normed = mixer_rows(
        head_inputs_unfiltered,
        group_write_vectors,
        group_read_vectors,
        output_gate_inputs,
        step_preactivation,
        extra_decay_logs,
        head_decay_logs,
        head_filter_taps,
        write_filter_taps,
        read_filter_taps,
        grouped_norm_gain,
    )
    tp_count = lax.axis_size("tp")
    tp_index = lax.axis_index("tp")
    ep_count = lax.axis_size(EP)
    tok_local = expert_input_rows.shape[0]
    model_width = expert_input_rows.shape[1]
    top_count = routes.shape[1]
    local_experts = routed_gate_weight.shape[0]
    experts = local_experts * ep_count
    capacity = 3 * tok_local * top_count // (2 * experts)
    rows_float = expert_input_rows.astype(jnp.float32)
    normed = (
        rows_float
        * lax.rsqrt(jnp.mean(rows_float * rows_float, axis=-1, keepdims=True) + eps_norm)
        * expert_norm_gain
    ).astype(jnp.bfloat16)
    group_rows, group_routes, group_scores = (
        lax.all_gather(normed, "tp", axis=0, tiled=True),
        lax.all_gather(routes, "tp", axis=0, tiled=True),
        lax.all_gather(router_chosen_scores, "tp", axis=0, tiled=True),
    )
    score_float = group_scores.astype(jnp.float32)
    weights = score_float / jnp.sum(score_float, axis=1, keepdims=True) * route_scale
    by_owner = group_routes.reshape(tp_count, tok_local * top_count)
    onehot = (by_owner[:, :, None] == jnp.arange(experts, dtype=jnp.int32)[None, None, :]).astype(
        jnp.int32
    )
    before = jnp.cumsum(onehot, axis=1) - onehot
    slot_rank = jnp.sum(before * onehot, axis=2)
    owner_base = jnp.arange(tp_count, dtype=jnp.int32)[:, None] * (experts * capacity)
    slot_index = owner_base + by_owner * capacity + slot_rank
    own_slot = lax.dynamic_index_in_dim(slot_index, tp_index, 0, keepdims=False) - tp_index * (
        experts * capacity
    )
    shared_hidden = (
        jax.nn.silu(jnp.dot(group_rows, shared_gate_weight, preferred_element_type=jnp.float32))
        * jnp.dot(group_rows, shared_up_weight, preferred_element_type=jnp.float32)
    ).astype(jnp.bfloat16)
    shared_part = jnp.dot(shared_hidden, shared_down_weight, preferred_element_type=jnp.float32)
    own_token = jnp.arange(tok_local * top_count, dtype=jnp.int32) // top_count
    own_table = jnp.full((experts * capacity,), tok_local, jnp.int32).at[own_slot].set(own_token)
    own_padded = jnp.concatenate([normed, jnp.zeros((1, model_width), jnp.bfloat16)], axis=0)
    own_out = own_padded[own_table].reshape(experts, capacity, model_width)
    own_arrived = lax.all_to_all(own_out, EP, split_axis=0, concat_axis=0, tiled=True)
    arrived = lax.all_gather(own_arrived[None], "tp", axis=0, tiled=True)
    sources = arrived.reshape(tp_count, ep_count, local_experts, capacity, model_width)
    gate_value = jnp.einsum(
        "osecd,edf->osecf", sources, routed_gate_weight, preferred_element_type=jnp.float32
    )
    up_value = jnp.einsum(
        "osecd,edf->osecf", sources, routed_up_weight, preferred_element_type=jnp.float32
    )
    hidden = (jax.nn.silu(gate_value) * up_value).astype(jnp.bfloat16)
    partial_value = jnp.einsum(
        "osecf,efd->osecd", hidden, routed_down_weight, preferred_element_type=jnp.float32
    ).astype(jnp.bfloat16)
    slot_rows = ep_count * local_experts * capacity
    flat_partial = partial_value.reshape(tp_count * slot_rows, model_width)
    summed = summed_on_arrival(flat_partial.astype(jnp.float32).astype(jnp.bfloat16), "tp", 0)
    returned_sums = lax.all_to_all(
        summed.reshape(ep_count * local_experts, capacity, model_width).astype(jnp.bfloat16),
        EP,
        split_axis=0,
        concat_axis=0,
        tiled=True,
    ).astype(jnp.float32)
    own_weights = lax.dynamic_slice_in_dim(weights, tp_index * tok_local, tok_local, 0)
    picked = returned_sums.reshape(-1, model_width)[own_slot].reshape(
        tok_local, top_count, model_width
    )
    own_term = jnp.sum(picked * own_weights[:, :, None], axis=1)
    mix_block = mixer_normed.shape[0] // tp_count
    block_rows = mix_block + tok_local
    part_count = block_rows * lax.axis_size("tp") // block_rows
    mix_term = jnp.dot(
        mixer_normed, mixer_output_weight, preferred_element_type=jnp.float32
    ).reshape(part_count, mix_block, model_width)
    moe_term = shared_part.reshape(part_count, tok_local, model_width)
    row_sums = summed_on_arrival(
        jnp.concatenate([mix_term, moe_term], axis=1)
        .reshape(block_rows * lax.axis_size("tp"), model_width)
        .astype(jnp.bfloat16),
        "tp",
        0,
    )
    mixer_result = row_sums[:mix_block].astype(jnp.bfloat16)
    moe_sum = row_sums[mix_block:]
    moe_total = moe_sum + own_term
    return (mixer_result, moe_total.astype(jnp.bfloat16))


def solution(mesh):
    split = Mesh(mesh.devices.reshape(8, 4, 2, mesh.shape["tp"]), ("ep_0", "ep_1", "ep_2", "tp"))
    placed = (
        P(EP, "tp"),
        P(EP, "tp"),
        P(EP, "tp"),
        P(EP, "tp"),
        P("tp", EP),
        P("tp", EP),
        P("tp"),
        P(None, "tp"),
        P(None, "tp"),
        P(None, "tp"),
        P("tp"),
        P("tp", None),
        P(EP_TP, None),
        P(),
        P(EP_TP, None),
        P(EP_TP, None),
        P(EP, None, "tp"),
        P(EP, None, "tp"),
        P(EP, "tp", None),
        P(None, "tp"),
        P(None, "tp"),
        P("tp", None),
    )
    return jax.shard_map(
        local,
        mesh=split,
        in_specs=placed,
        out_specs=(P(EP_TP, None), P(EP_TP, None)),
        check_vma=False,
    )
```

profile of v0, /device:TPU:1, one launch (start us, length us, event | category | flops | bytes accessed | tf_op | source)
XLA Modules:
  0.0 428.6 jit_solution(2812182041163387984)
XLA Ops:
  9.5 4.5 %collective-permute-start = (bf16[3,1280]{1,0:T(4,128)(2,1)S(1)}, bf16[3,1280]{1,0:T(4,128)(2,1)S(1)}, u32[]{:S(2)}, u32[]{:S(2)}) collective-permute-start(bf16[3,1280]{1,0:T(4,128)(2,1)S(1)} %pad_maximum_fusion.4), channel_id=1, source_target_pairs={{0,4},{4,8},{8,12},{12,16},{16,20},{20,24},{24,28},{28,32},{32,36}... | collective-permute-start | bytes 23048 | tf_op jit(solution)/shard_map/ppermute | solution.py:22
  14.0 8.2 %all_gather.45 = s32[512,2]{0,1:T(2,128)S(1)} all-gather(s32[128,2]{0,1:T(2,128)} %param.36), channel_id=1, replica_groups=mesh['ep_0'=8,'ep_1'=4,'ep_2'=2,'tp'=4] {'tp'}, dimensions={0}, use_global_device_ids=true | all-gather | bytes 5120 | tf_op jit(solution)/shard_map/all_gather | solution.py:232
  23.5 0.9 slice_convert_fusion.4
  26.7 1.2 fusion.23
  28.0 2.4 reduce-window.6
  32.1 2.2 all-gather.1
  34.5 1.4 scatter_custom_fusion
  37.1 1.1 fusion.30
  38.2 1.1 copy-done.11
  39.3 4.5 %fusion.38 = f32[16,1,64,128]{3,1,2,0:T(1,128)} fusion(f32[16,2,1,1]{1,2,3,0:T(1,128)S(1)} %copy.77, f32[2,16,64,128]{3,2,1,0:T(8,128)S(1)} %fusion.30), kind=kOutput, calls=%fused_computation.51 | convolution fusion | flops 3145728 | bytes 1572992 | tf_op jit(solution)/shard_map/gec,cgepn->gepn/dot_general | solution.py:147
  44.2 15.3 %all-gather.16.cloned.1.call-done = f32[32,64,128]{2,1,0:T(8,128)} async-done(((f32[16,64,128]{2,1,0:T(8,128)}), f32[32,64,128]{2,1,0:T(8,128)}) %all-gather.16.cloned.1.call-update) | async-done | bytes 1048592 | tf_op jit(solution)/shard_map/all_gather | solution.py:36
  59.5 2.2 fusion.54
  61.9 3.1 gather_fusion
  65.0 2.5 reshape.640
  67.5 59.4 %all_to_all.20 = bf16[64,6,2048]{2,1,0:T(8,128)(2,1)S(1)} all-to-all(bf16[64,6,2048]{2,1,0:T(8,128)(2,1)S(1)} %reshape.640), channel_id=1, replica_groups=mesh['ep_0'=8,'ep_1'=4,'ep_2'=2,'tp'=4] {'ep_0','ep_1','ep_2'}, dimensions={0} | all-to-all | bytes 3145728 | tf_op jit(solution)/shard_map/all_to_all | solution.py:257
  126.9 2.0 copy.69
  130.1 7.5 %all-gather.3 = f32[4,16,1]{1,2,0:T(1,128)S(1)} all-gather(f32[1,16,1]{1,2,0:T(1,128)S(1)} %get-tuple-element.4), channel_id=5, replica_groups=mesh['ep_0'=8,'ep_1'=4,'ep_2'=2,'tp'=4] {'ep_1'}, dimensions={0}, use_global_device_ids=true | all-gather | bytes 320 | tf_op jit(solution)/shard_map/all_gather | solution.py:36
  137.6 2.7 slice_add_fusion.12
  141.2 53.5 %all-gather.18.cloned.1.call-done = bf16[256,6,2048]{2,0,1:T(8,128)(2,1)} async-done(((bf16[64,6,2048]{2,0,1:T(8,128)(2,1)}), bf16[256,6,2048]{2,0,1:T(8,128)(2,1)}) %all-gather.18.cloned.1.call-update) | async-done | bytes 6291472 | tf_op jit(solution)/shard_map/all_gather | solution.py:258
  194.7 5.7 %fusion.2 = f32[4,64,6,256]{3,1,2,0:T(8,128)} fusion(bf16[4,64,6,2048]{3,1,0,2:T(8,128)(2,1)} %bitcast.287, bf16[1,2048,256]{2,1,0:T(8,128)(2,1)S(1)} %copy-done.37), kind=kOutput, calls=%fused_computation.6 | convolution fusion | flops 1610612736 | bytes 8912896 | tf_op jit(solution)/shard_map/osecd,edf->osecf/dot_general | solution.py:260
  200.5 12.6 %convert_bitcast_fusion = bf16[4,64,1,6,2048]{4,1,3,0,2:T(8,128)(2,1)} fusion(bf16[1,256,2048]{2,1,0:T(8,128)(2,1)S(1)} %copy-done, bf16[4,64,6,2048]{3,1,0,2:T(8,128)(2,1)} %bitcast.288, f32[4,64,6,256]{3,1,2,0:T(8,128)} %fusion.2, bf16[1,2048,256]{2,1,0:T(8,128)(2,1)} %param.39), kind=kOutput, calls=%fused_computation.3 | convolution fusion | flops 3226730496 | bytes 16252928 | tf_op jit(solution)/shard_map/osecf,efd->osecd/dot_general | solution.py:267
  213.1 18.3 %copy.72 = bf16[4,64,1,6,2048]{4,0,3,1,2:T(4,128)(2,1)S(1)} copy(bf16[4,64,1,6,2048]{4,1,3,0,2:T(8,128)(2,1)} %convert_bitcast_fusion) | data formatting | bytes 12582912 | tf_op jit(solution)/shard_map/convert_element_type | solution.py:269
  231.4 6.1 %copy.73 = bf16[4,384,2048]{2,1,0:T(8,128)(2,1)} copy(bf16[4,384,2048]{2,0,1:T(4,128)(2,1)S(1)} %bitcast.267) | data formatting | bytes 12582912 | tf_op jit(solution)/shard_map/reshape | solution.py:48
  237.5 5.4 %all-to-all-start.2 = ((bf16[4,384,2048]{2,1,0:T(8,128)(2,1)}), bf16[4,384,2048]{2,1,0:T(8,128)(2,1)}, u32[]{:S(2)}, u32[]{:S(2)}) async-start(bf16[4,384,2048]{2,1,0:T(8,128)(2,1)} %copy.73), calls=%async_computation.2 | async-start | bytes 12582912 | tf_op jit(solution)/shard_map/all_to_all | solution.py:53
  245.0 14.8 %all_gather.43 = f32[8,1,16]{2,1,0:T(1,128)S(1)} all-gather(f32[1,1,16]{2,1,0:T(1,128)S(1)} %get-tuple-element.6), channel_id=1, replica_groups=mesh['ep_0'=8,'ep_1'=4,'ep_2'=2,'tp'=4] {'ep_0'}, dimensions={0}, use_global_device_ids=true | all-gather | bytes 576 | tf_op jit(solution)/shard_map/all_gather | solution.py:36
  262.6 2.3 fusion.116
  264.9 5.7 %convolution_convert_fusion = bf16[512,2048]{1,0:T(8,128)(2,1)} fusion(bf16[128,2048]{1,0:T(8,128)(2,1)} %param.43, bf16[512,2048]{1,0:T(8,128)(2,1)} %all-gather.14.cloned.1.call-done, bf16[2048,128]{1,0:T(8,128)(2,1)} %param.42, f32[512,128]{1,0:T(8,128)S(1)} %fusion.116), kind=kOutput, calls=%fused_computation.11 | convolution fusion | flops 538312704 | bytes 5505024 | tf_op jit(solution)/shard_map/dot_general | solution.py:252
  270.6 16.9 %all-gather.12.cloned.1.call-done = f32[8,1,16,64,128]{4,3,2,1,0:T(8,128)} async-done(((f32[1,1,16,64,128]{4,3,2,1,0:T(8,128)}), f32[8,1,16,64,128]{4,3,2,1,0:T(8,128)}) %all-gather.12.cloned.1.call-update) | async-done | bytes 4194320 | tf_op jit(solution)/shard_map/all_gather | solution.py:36
  287.5 3.1 fusion.52
  290.7 4.2 fusion.21
  295.0 1.0 fusion.16
  296.1 2.0 fusion.15
  299.6 3.1 fusion.6
  302.7 1.6 pad_maximum_fusion
  304.3 9.1 %all-to-all-done.2 = bf16[4,384,2048]{2,1,0:T(8,128)(2,1)} async-done(((bf16[4,384,2048]{2,1,0:T(8,128)(2,1)}), bf16[4,384,2048]{2,1,0:T(8,128)(2,1)}, u32[]{:S(2)}, u32[]{:S(2)}) %all-to-all-start.2) | async-done | bytes 6291488 | tf_op jit(solution)/shard_map/all_to_all | solution.py:53
  313.5 3.9 all-to-all-start
  317.3 5.7 %reduce_sum.70 = bf16[384,2048]{1,0:T(8,128)(2,1)} reduce(bf16[4,384,2048]{2,1,0:T(8,128)(2,1)} %all-to-all-done.2, bf16[]{:T(256)} %constant.109.clone.1), dimensions={0}, to_apply=%region_9.10 | reduce | flops 2359296 | bytes 7864322 | tf_op jit(solution)/shard_map/reduce_sum | solution.py:54
  323.0 3.7 convert_element_type.143
  326.7 21.0 %all-to-all-done = bf16[4,160,2048]{2,1,0:T(8,128)(2,1)S(1)} async-done(((bf16[4,160,2048]{2,1,0:T(8,128)(2,1)}), bf16[4,160,2048]{2,1,0:T(8,128)(2,1)S(1)}, u32[]{:S(2)}, u32[]{:S(2)}) %all-to-all-start) | async-done | bytes 2621472 | tf_op jit(solution)/shard_map/all_to_all | solution.py:53
  347.6 12.7 %all-to-all-start.3 = ((bf16[64,6,2048]{2,1,0:T(8,128)(2,1)}), bf16[64,6,2048]{2,1,0:T(8,128)(2,1)}, u32[]{:S(2)}, u32[]{:S(2)}) async-start(bf16[64,6,2048]{2,1,0:T(8,128)(2,1)} %convert_element_type.143), calls=%async_computation.3 | async-start | bytes 4194304 | tf_op jit(solution)/shard_map/all_to_all | solution.py:273
  360.4 6.9 %all_gather.47 = bf16[512,2]{0,1:T(2,128)(2,1)S(1)} all-gather(bf16[128,2]{0,1:T(2,128)(2,1)S(1)} %copy-done.36), channel_id=1, replica_groups=mesh['ep_0'=8,'ep_1'=4,'ep_2'=2,'tp'=4] {'tp'}, dimensions={0}, use_global_device_ids=true | all-gather | bytes 2560 | tf_op jit(solution)/shard_map/all_gather | solution.py:233
  368.0 1.1 copy-done.6
  369.8 40.2 %all-to-all-done.3 = bf16[64,6,2048]{2,1,0:T(8,128)(2,1)} async-done(((bf16[64,6,2048]{2,1,0:T(8,128)(2,1)}), bf16[64,6,2048]{2,1,0:T(8,128)(2,1)}, u32[]{:S(2)}, u32[]{:S(2)}) %all-to-all-start.3) | async-done | bytes 1572896 | tf_op jit(solution)/shard_map/all_to_all | solution.py:273
  410.0 2.5 reshape.664
  412.5 2.7 gather_fusion.1
  415.2 2.5 reshape.648
  417.8 3.2 multiply_reduce_fusion
  421.0 0.9 fusion.26
  (163 shorter events, 19.2 us)
Async XLA Ops:
  7.2 193.3 %copy-start = (bf16[1,256,2048]{2,1,0:T(8,128)(2,1)S(1)}, bf16[1,256,2048]{2,1,0:T(8,128)(2,1)}, u32[]{:S(2)}) copy-start(bf16[1,256,2048]{2,1,0:T(8,128)(2,1)} %param.40) | copy-start | bytes 3145732
  7.2 28.7 %copy-start.15 = (bf16[128,1024]{1,0:T(8,128)(2,1)S(1)}, bf16[128,1024]{1,0:T(8,128)(2,1)}, u32[]{:S(2)}) copy-start(bf16[128,1024]{1,0:T(8,128)(2,1)} %param.22) | copy-start | bytes 786436
  7.2 52.3 %all-gather.16.cloned.1.call-start = ((), (), s32[]{:S(2)}) async-start(), calls=%async_computation.7 | async-start | bytes 1572864 | tf_op jit(solution)/shard_map/all_gather | solution.py:36
  9.5 26.4 %collective-permute-start = (bf16[3,1280]{1,0:T(4,128)(2,1)S(1)}, bf16[3,1280]{1,0:T(4,128)(2,1)S(1)}, u32[]{:S(2)}, u32[]{:S(2)}) collective-permute-start(bf16[3,1280]{1,0:T(4,128)(2,1)S(1)} %pad_maximum_fusion.4), channel_id=1, source_target_pairs={{0,4},{4,8},{8,12},{12,16},{16,20},{20,24},{24,28},{28,32},{32,36}... | collective-permute-start | bytes 23048 | tf_op jit(solution)/shard_map/ppermute | solution.py:22
  32.1 4.9 %copy-start.34 = (s32[256,1]{0,1:T(1,128)}, s32[256,1]{0,1:T(1,128)S(1)}, u32[]{:S(2)}) copy-start(s32[256,1]{0,1:T(1,128)S(1)} %compare_select_fusion.1) | copy-start | bytes 3076
  34.4 2.7 copy-start.16
  35.9 1.1 copy-start.20
  37.0 6.8 %copy-start.2 = (f32[2,64,16,64]{1,3,2,0:T(8,128)}, f32[2,64,16,64]{1,3,2,0:T(8,128)S(1)}, u32[]{:S(2)}) copy-start(f32[2,64,16,64]{1,3,2,0:T(8,128)S(1)} %copy.55) | copy-start | bytes 1572868
  37.1 6.8 %copy-start.10 = (bf16[128,2048]{1,0:T(8,128)(2,1)S(1)}, bf16[128,2048]{1,0:T(8,128)(2,1)}, u32[]{:S(2)}) copy-start(bf16[128,2048]{1,0:T(8,128)(2,1)} %param.34) | copy-start | bytes 1572868
  37.1 6.8 %copy-start.23 = (f32[2048]{0:T(1024)S(1)}, f32[2048]{0:T(1024)}, u32[]{:S(2)}) copy-start(f32[2048]{0:T(1024)} %param.35) | copy-start | bytes 24580
  38.2 1.1 copy-start.11
  43.8 93.8 %all-gather.10.cloned.1.call-start = ((), (), s32[]{:S(2)}) async-start(), calls=%async_computation.4 | async-start | bytes 2621440 | tf_op jit(solution)/shard_map/all_gather | solution.py:36
  43.9 17.9 %copy-start.27 = (f32[16]{0:T(128)}, f32[16]{0:T(128)S(1)}, u32[]{:S(2)}) copy-start(f32[16]{0:T(128)S(1)} %get-tuple-element.27) | copy-start | bytes 196
  43.9 17.9 %copy-start.28 = (f32[16]{0:T(128)}, f32[16]{0:T(128)S(1)}, u32[]{:S(2)}) copy-start(f32[16]{0:T(128)S(1)} %get-tuple-element.28) | copy-start | bytes 196
  44.2 17.7 %copy-start.8 = (bf16[128,2048]{1,0:T(8,128)(2,1)}, bf16[128,2048]{1,0:T(8,128)(2,1)S(1)}, u32[]{:S(2)}) copy-start(bf16[128,2048]{1,0:T(8,128)(2,1)S(1)} %fusion.25) | copy-start | bytes 1572868
  61.7 133.0 %all-gather.18.cloned.1.call-start = ((), (), s32[]{:S(2)}) async-start(), calls=%async_computation.8 | async-start | bytes 7864320 | tf_op jit(solution)/shard_map/all_gather | solution.py:258
  128.9 65.8 %copy-start.37 = (bf16[1,2048,256]{2,1,0:T(8,128)(2,1)S(1)}, bf16[1,2048,256]{2,1,0:T(8,128)(2,1)}, u32[]{:S(2)}) copy-start(bf16[1,2048,256]{2,1,0:T(8,128)(2,1)} %param.38) | copy-start | bytes 3145732
  129.0 133.6 %all-gather.14.cloned.1.call-start = ((), (), s32[]{:S(2)}) async-start(), calls=%async_computation.6 | async-start | bytes 2621440 | tf_op jit(solution)/shard_map/all_gather | solution.py:231
  129.5 158.0 %all-gather.12.cloned.1.call-start = ((), (), s32[]{:S(2)}) async-start(), calls=%async_computation.5 | async-start | bytes 4718592 | tf_op jit(solution)/shard_map/all_gather | solution.py:36
  137.6 2.8 copy-start.29
  137.6 2.8 copy-start.30
  137.6 2.8 copy-start.31
  137.6 2.8 copy-start.32
  237.5 23.6 %copy-start.33 = (bf16[4,128]{1,0:T(4,128)(2,1)S(1)}, bf16[4,128]{1,0:T(4,128)(2,1)}, u32[]{:S(2)}) copy-start(bf16[4,128]{1,0:T(4,128)(2,1)} %param.31) | copy-start | bytes 3076
  237.5 24.8 %copy-start.21 = (bf16[128,128]{1,0:T(8,128)(2,1)S(1)}, bf16[128,128]{1,0:T(8,128)(2,1)}, u32[]{:S(2)}) copy-start(bf16[128,128]{1,0:T(8,128)(2,1)} %param.24) | copy-start | bytes 98308
  237.5 25.1 %copy-start.14 = (bf16[2048,128]{1,0:T(8,128)(2,1)S(1)}, bf16[2048,128]{1,0:T(8,128)(2,1)}, u32[]{:S(2)}) copy-start(bf16[2048,128]{1,0:T(8,128)(2,1)} %param.41) | copy-start | bytes 1572868
  237.5 76.0 %all-to-all-start.2 = ((bf16[4,384,2048]{2,1,0:T(8,128)(2,1)}), bf16[4,384,2048]{2,1,0:T(8,128)(2,1)}, u32[]{:S(2)}, u32[]{:S(2)}) async-start(bf16[4,384,2048]{2,1,0:T(8,128)(2,1)} %copy.73), calls=%async_computation.2 | async-start | bytes 12582912 | tf_op jit(solution)/shard_map/all_to_all | solution.py:53
  264.9 22.6 %copy-start.4 = (f32[4,1,16,64,128]{4,3,2,1,0:T(8,128)S(1)}, f32[4,1,16,64,128]{4,3,2,1,0:T(8,128)}, u32[]{:S(2)}) copy-start(f32[4,1,16,64,128]{4,3,2,1,0:T(8,128)} %all-gather.10.cloned.1.call-done) | copy-start | bytes 6291460
  264.9 22.6 %copy-start.9 = (f32[32,64,128]{2,1,0:T(8,128)S(1)}, f32[32,64,128]{2,1,0:T(8,128)}, u32[]{:S(2)}) copy-start(f32[32,64,128]{2,1,0:T(8,128)} %all-gather.16.cloned.1.call-done) | copy-start | bytes 3145732
  287.5 3.1 copy-start.12
  287.5 3.1 copy-start.24
  287.5 3.1 copy-start.25
  287.5 3.1 copy-start.26
  287.5 3.1 copy-start.38
  290.6 4.3 %copy-start.19 = (f32[2,64,16]{1,2,0:T(8,128)S(1)}, f32[2,64,16]{1,2,0:T(8,128)}, u32[]{:S(2)}) copy-start(f32[2,64,16]{1,2,0:T(8,128)} %exponential_bitcast_fusion) | copy-start | bytes 24580
  294.9 1.2 copy-start.3
  294.9 1.2 copy-start.17
  294.9 1.2 copy-start.22
  298.2 1.0 copy-start.13
  298.7 0.9 copy-start.18
  299.6 3.1 copy-start.5
  313.5 34.2 %all-to-all-start = ((bf16[4,160,2048]{2,1,0:T(8,128)(2,1)}), bf16[4,160,2048]{2,1,0:T(8,128)(2,1)S(1)}, u32[]{:S(2)}, u32[]{:S(2)}) async-start(bf16[4,160,2048]{2,1,0:T(8,128)(2,1)} %pad_maximum_fusion), calls=%async_computation | async-start | bytes 5242880 | tf_op jit(solution)/shard_map/all_to_all | solution.py:53
  326.7 33.7 %copy-start.36 = (bf16[128,2]{0,1:T(2,128)(2,1)S(1)}, bf16[128,2]{0,1:T(2,128)(2,1)}, u32[]{:S(2)}) copy-start(bf16[128,2]{0,1:T(2,128)(2,1)} %param.37) | copy-start | bytes 1540
  326.7 40.9 %copy-start.35 = (s32[256,1]{0,1:T(1,128)S(1)}, s32[256,1]{0,1:T(1,128)}, u32[]{:S(2)}) copy-start(s32[256,1]{0,1:T(1,128)} %copy-done.34) | copy-start | bytes 3076
  347.6 62.4 %all-to-all-start.3 = ((bf16[64,6,2048]{2,1,0:T(8,128)(2,1)}), bf16[64,6,2048]{2,1,0:T(8,128)(2,1)}, u32[]{:S(2)}, u32[]{:S(2)}) async-start(bf16[64,6,2048]{2,1,0:T(8,128)(2,1)} %convert_element_type.143), calls=%async_computation.3 | async-start | bytes 4194304 | tf_op jit(solution)/shard_map/all_to_all | solution.py:273
  368.0 1.1 copy-start.6
  417.7 3.2 copy-start.7
  417.7 4.1 copy-start.1
Sparse Core Ops, SparseCore 0:
  43.9 15.5 all-gather.15
  61.8 49.1 all-gather.9
  129.1 65.6 all-gather.17
  197.0 33.9 all-gather.13
  232.6 54.8 all-gather.11
where the time goes:
time: 433 us; the launch traced here: 429 us
  waiting for transfers between devices  157 us (36%)
  blocking collectives  99 us (23%)
  local copies, waits for them, and re-layouts  56.7 us (13%)
  matrix products  42.5 us (10%)
  other arithmetic  32.3 us (7%)
  starting transfers between devices  26.7 us (6%)
  between operations  14.9 us (3%)
    all_to_all x1, blocking collectives, local(): lax.all_to_all(own_out, EP, split_axis=0, concat_axis=0, tiled=True)  59.4 us
    all_gather x1, waiting for transfers between devices, local(): arrived = lax.all_gather(own_arrived[None], 'tp', axis=0, tiled=True)  53.5 us
    all_to_all x1, waiting for transfers between devices, local(): lax.all_to_all(summed.reshape(ep_count * local_experts, capacity, model_w...  40.2 us
    all_gather x3, waiting for transfers between devices, entering_2(): pieces = jax.tree.map(lambda part: lax.all_gather(part, axis), running)  32.2 us
    all_to_all x2, waiting for transfers between devices, summed_on_arrival(): lax.all_to_all(split_up(value, dim, devices), axis, 0, 0, tiled=True)  30.1 us
    all_gather x3, blocking collectives, entering_2(): pieces = jax.tree.map(lambda part: lax.all_gather(part, axis), running)  24.5 us
    convert_element_type x1, local copies, waits for them, and re-layouts, local(): partial_value = jnp.einsum('osecf,efd->osecd', hidden, routed_down_weight...  18.3 us
    all_to_all x1, starting transfers between devices, local(): lax.all_to_all(summed.reshape(ep_count * local_experts, capacity, model_w...  12.7 us
  transfers between devices with their start and end apart: 9, of which 6 were waited for; matrix products, arithmetic and copies ran while one was open for 25% of the time, Pallas kernels for 0%

commit v1 on v0

v1 whole, which is shorter than its diff:
```python
import jax
import jax.numpy as jnp
import numpy as np
from jax import lax
from jax.experimental import pallas as pl
from jax.experimental.pallas import tpu as pltpu
from jax.sharding import Mesh
from jax.sharding import PartitionSpec as P

HEAD_DIM = 64
STATE = 128
CAP = 6
SIZES = (128, 256, 256, 256, 256, 256, 256, 256, 128)
CHUNKS = len(SIZES)
COLS = tuple(slice(sum(SIZES[:c]), sum(SIZES[: c + 1])) for c in range(CHUNKS))
Z, X, G, Y = 8, 4, 8, 4
EP = ("ep_0", "ep_1", "ep_2")
EP_TP = ("ep_0", "ep_1", "ep_2", "tp")
MESH = pl.DeviceIdType.MESH

eps_norm = 1e-06
route_scale = 2.5
highest = lax.Precision.HIGHEST
f32 = jnp.float32
bf16 = jnp.bfloat16


class Names:
    def __init__(self, names, refs):
        self.__dict__.update(zip(names, refs))


def dot(a, b, precision=None):
    return jnp.dot(a, b, preferred_element_type=f32, precision=precision)


def dot_t(a, b, precision=None):
    return lax.dot_general(
        a, b, (((0,), (0,)), ((), ())), preferred_element_type=f32, precision=precision
    )


def silu(v):
    return v * (1.0 / (1.0 + jnp.exp(-v)))


def make_kernel(inputs, scratch):
    def kernel(*refs):
        n = len(inputs)
        body(Names(inputs, refs[:n]), refs[n], refs[n + 1], Names(scratch, refs[n + 2 :]))

    return kernel


def body(i, mix_out, moe_out, s):
    z = lax.axis_index("ep_0")
    x = lax.axis_index("ep_1")
    core = lax.axis_index("ep_2")
    y = lax.axis_index("tp")
    g = x * 2 + core
    ep = z * G + g
    width = i.rows.shape[1]
    ff = i.gate_w.shape[2]
    tok = i.rows.shape[0]
    slots = Z * G * CAP
    zrows = G * CAP
    n_pos = i.heads.shape[0]
    chans = i.heads.shape[1]
    heads = i.step.shape[0]
    per = chans // G

    def z_peer(d):
        return (lax.rem(z + d, Z), x, core, y)

    def g_peer(d):
        t = lax.rem(g + d, G)
        return (z, lax.div(t, 2), lax.rem(t, 2), y)

    def x_peer(d):
        return (z, lax.rem(x + d, X), core, y)

    def y_peer(d):
        return (z, x, core, lax.rem(y + d, Y))

    def ep_peer(d):
        t = lax.rem(ep + d + Z * G, Z * G)
        r = lax.rem(t, G)
        return (lax.div(t, G), lax.div(r, 2), lax.rem(r, 2), y)

    pair_y = y + 1 - 2 * lax.rem(y, 2)
    weight_pair = (z, x, core, pair_y)
    token_pair = (z, x, core, Y - 1 - y)
    sibling = (z, x, 1 - core, y)

    def rc(src, dst, send, recv, dev):
        return pltpu.make_async_remote_copy(
            src_ref=src, dst_ref=dst, send_sem=send, recv_sem=recv, device_id=dev, device_id_type=MESH
        )

    def drain(ref, sem):
        pltpu.make_async_copy(ref, ref, sem).wait()

    barrier = pltpu.get_barrier_semaphore()

    def greet(dev):
        pl.semaphore_signal(barrier, inc=1, device_id=dev, device_id_type=MESH)

    @pl.loop(1, Z)
    def _(d):
        greet(z_peer(d))
        greet(g_peer(d))

    @pl.loop(1, Y)
    def _(d):
        greet(y_peer(d))

    greet(ep_peer(1))
    greet(ep_peer(-1))

    def tail_copies():
        last = pl.ds(n_pos - 16, 16)
        dev = ep_peer(1)
        return [
            rc(src.at[last, :], dst, s.tail_s.at[k], s.tail_r.at[k], dev)
            for k, (src, dst) in enumerate(
                ((i.heads, s.tail_heads), (i.write, s.tail_write), (i.read, s.tail_read))
            )
        ]

    def weight_copy(k, c):
        src = (i.gate_w, i.up_w, i.down_w)[k].at[0]
        if k < 2:
            src, dst = src.at[COLS[c], :], s.pgu.at[k, COLS[c], :]
        else:
            src, dst = src.at[:, COLS[c]], s.pdown.at[:, COLS[c]]
        return rc(src, dst, s.w_s.at[k // 2], s.w_r.at[k // 2, c], weight_pair)

    shared_full = (s.full_gate, s.full_up, s.full_down)

    def piece(t, slot, q, count=1):
        ref = shared_full[t]
        n = ref.shape[1] // G
        return ref.at[slot, pl.ds(pl.multiple_of(q * n, n), count * n), :]

    def sh_y(t):
        q = core * X + x
        return rc(piece(t, 0, q), piece(t, 1, q), s.shy_s.at[t], s.shy_r.at[t], token_pair)

    def sh_x_start(t, d):
        part = piece(t, 1, core * X + x)
        rc(part, part, s.shx_s.at[t], s.shx_r.at[t], x_peer(d)).start()

    def sh_x_drain(t, sem):
        drain(piece(t, 1, 0, X - 1), sem.at[t])

    def sh_c(t):
        part = piece(t, 1, core * X, X)
        return rc(part, part, s.shc_s.at[t], s.shc_r.at[t], sibling)

    def shared_rows():
        return rc(s.normed, s.pair_normed, s.st_s.at[0], s.st_r.at[0], weight_pair)

    def shared_return():
        return rc(s.sh_send, s.sh_recv, s.st_s.at[1], s.st_r.at[1], weight_pair)

    def sy(c):
        part = (slice(None), slice(None), COLS[c])
        return rc(s.toks.at[0].at[part], s.toks.at[1].at[part], s.y_s.at[0], s.y_r.at[0, c], token_pair)

    def ry(c):
        return rc(s.ysend.at[:, COLS[c]], s.yrecv.at[:, COLS[c]], s.y_s.at[1], s.y_r.at[1, c], token_pair)

    def spread_z(src, dst, c, k):
        @pl.loop(1, Z)
        def _(d):
            rc(
                src.at[lax.rem(z + d, Z), :, COLS[c]], dst.at[z, :, COLS[c]], s.z_s.at[k], s.z_r.at[k, c], z_peer(d)
            ).start()

    def spread_g(src, dst, c, k):
        @pl.loop(1, G)
        def _(d):
            rc(
                src.at[lax.rem(g + d, G), :, COLS[c]], dst.at[g, :, COLS[c]], s.g_s.at[k], s.g_r.at[k, c], g_peer(d)
            ).start()

    def seven(ref, c, sem, k):
        drain(ref.at[pl.ds(0, 7), :, COLS[c]], sem.at[k, c])

    def mix_g(src, dst, k, d):
        rc(src.at[lax.rem(g + d, G)], dst.at[g], s.m_s.at[k], s.m_r.at[k], g_peer(d)).start()

    def mix_drain(ref, sem, k):
        drain(ref.at[pl.ds(0, 7)], sem.at[k])

    bring = []

    def fetched(src, dst):
        bring.append((src, dst))
        return pltpu.make_async_copy(src, dst, s.loc.at[len(bring) - 1])

    small_in = [
        fetched(src, dst)
        for src, dst in (
            (i.routes, s.routes),
            (i.scores, s.scores),
            (i.row_gain, s.row_gain),
            (i.rows, s.rows),
            (i.write, s.write),
            (i.read, s.read),
            (i.step, s.step),
            (i.extra, s.extra),
            (i.decay, s.decay),
            (i.head_taps, s.head_taps),
            (i.write_taps, s.write_taps),
            (i.read_taps, s.read_taps),
            (i.mix_gain, s.mix_gain),
        )
    ]
    local = dict(
        heads=fetched(i.heads, s.heads),
        gates=fetched(i.gates, s.gates),
        perm=fetched(i.perm, s.perm),
        sh_gate=fetched(i.sh_gate, s.full_gate.at[0]),
        sh_up=fetched(i.sh_up, s.full_up.at[0]),
        sh_down=fetched(i.sh_down, s.full_down.at[0]),
        gate=fetched(i.gate_w.at[0], s.ogate),
        up=fetched(i.up_w.at[0], s.oup),
        down=fetched(i.down_w.at[0], s.odown),
        mixw=fetched(i.mix_weight, s.mixw),
    )
    for copy in small_in + list(local.values()):
        copy.start()
    local = Names(local.keys(), local.values())
    for copy in small_in[:4]:
        copy.wait()
    route = s.routes[...]
    score = s.scores[...].astype(f32)
    weight = score / jnp.sum(score, axis=0, keepdims=True) * route_scale
    expert_iota = lax.broadcasted_iota(jnp.int32, (Z * G, tok), 0)
    hot = [(route[k : k + 1, :] == expert_iota).astype(f32) for k in range(2)]
    earlier = (
        lax.broadcasted_iota(jnp.int32, (tok, tok), 0) < lax.broadcasted_iota(jnp.int32, (tok, tok), 1)
    ).astype(bf16)
    before = dot((hot[0] + hot[1]).astype(bf16), earlier)
    slot_iota = lax.broadcasted_iota(jnp.int32, (slots, tok), 0)
    pick = jnp.zeros((slots, tok), f32)
    pick_w = jnp.zeros((slots, tok), f32)
    for k in range(2):
        rank = jnp.sum(before * hot[k], axis=0, keepdims=True).astype(jnp.int32)
        here = slot_iota == route[k : k + 1, :] * CAP + rank
        pick = pick + here.astype(f32)
        pick_w = pick_w + jnp.where(here, weight[k : k + 1, :], 0.0)
    s.pick_w[...] = pick_w
    pick = pick.astype(bf16)
    rows = s.rows[...].astype(f32)
    normed = (
        rows * lax.rsqrt(jnp.mean(rows * rows, axis=1, keepdims=True) + eps_norm) * s.row_gain[...]
    ).astype(bf16)
    s.normed[...] = normed
    pl.semaphore_wait(barrier, (Z - 1) + (G - 1) + (Y - 1) + 2)

    def select(c):
        part = dot(pick, s.normed[:, COLS[c]]).astype(bf16)
        s.own[:, :, COLS[c]] = part.reshape(Z, zrows, -1)
        spread_z(s.own, s.recv1, c, 0)

    weight_copy(0, 0).start()
    weight_copy(1, 0).start()
    select(0)
    for copy in tail_copies():
        copy.start()
    for t in range(3):
        (local.sh_gate, local.sh_up, local.sh_down)[t].wait()
        sh_y(t).start()
    for c in range(1, CHUNKS):
        weight_copy(0, c).start()
        weight_copy(1, c).start()
        select(c)
    for c in range(CHUNKS):
        weight_copy(2, c).start()
    shared_rows().start()
    s.recv1[z] = s.own[z]

    ext = s.ext

    def mixer_conv():
        local.heads.wait()
        for copy in tail_copies():
            copy.wait_recv()
        has_before = (ep > 0).astype(f32)
        for copy in small_in[4:]:
            copy.wait()
        col = 0
        for src, tail in ((s.heads, s.tail_heads), (s.write, s.tail_write), (s.read, s.tail_read)):
            w = src.shape[1]
            ext[0:16, col : col + w] = tail[...].astype(f32) * has_before
            ext[16 : 16 + n_pos, col : col + w] = src[...].astype(f32)
            col += w

        def conv(taps_ref, col):
            w = taps_ref.shape[1]
            taps = taps_ref[...].astype(f32)
            total = jnp.zeros((n_pos, w), f32)
            for j in range(taps.shape[0]):
                total = total + taps[j : j + 1, :] * ext[13 + j : 13 + j + n_pos, col : col + w]
            return silu(total)

        s.hv[...] = conv(s.head_taps, 0)
        s.wv[...] = conv(s.write_taps, chans)
        s.rv[...] = conv(s.read_taps, chans + STATE)

    def row_col():
        return (
            lax.broadcasted_iota(jnp.int32, (n_pos, n_pos), 0),
            lax.broadcasted_iota(jnp.int32, (n_pos, n_pos), 1),
        )

    def mixer_states():
        pre = s.step[...]
        step = jnp.maximum(pre, 0.0) + jnp.log1p(jnp.exp(-jnp.abs(pre)))
        eye = lax.broadcasted_iota(jnp.int32, (heads, heads), 0) == lax.broadcasted_iota(
            jnp.int32, (heads, heads), 1
        )
        decay = jnp.sum(jnp.where(eye, s.decay[...], 0.0), axis=1, keepdims=True)
        rate = -jnp.exp(decay) * step + s.extra[...]
        pos_r, pos_c = row_col()
        cum = dot(rate, (pos_r <= pos_c).astype(f32), highest)
        s.cum[...] = cum
        total_decay = cum[:, n_pos - 1 : n_pos]
        lane = lax.broadcasted_iota(jnp.int32, (heads, chans), 1)
        first = lax.broadcasted_iota(jnp.int32, (heads, chans), 0) * HEAD_DIM
        spread = ((lane >= first) & (lane < first + HEAD_DIM)).astype(f32)
        xw = s.hv[...] * dot_t(step, spread, highest)
        s.hv[...] = xw
        s.cum_x[...] = dot_t(jnp.exp(cum), spread, highest)
        xe = xw * dot_t(jnp.exp(total_decay - cum), spread, highest)
        decay_x = dot_t(jnp.broadcast_to(total_decay, (heads, 8)), spread, highest)
        states = dot_t(s.wv[...], xe, highest)
        for j in range(G):
            s.st_send[j] = states[:, j * per : (j + 1) * per].astype(bf16)
            s.dec_send[j] = decay_x[:, j * per : (j + 1) * per]
        s.st_got[g] = s.st_send[g]
        s.dec_got[g] = s.dec_send[g]
        s.affinity[...] = lax.dot_general(
            s.rv[...], s.wv[...], (((1,), (1,)), ((), ())), preferred_element_type=f32, precision=highest
        )

    def mixer_scan(pairs):
        cum = s.cum[...]
        cum_t = jnp.transpose(cum)
        affinity = s.affinity[...]
        pos_r, pos_c = row_col()
        low = pos_r >= pos_c
        pair_lane = lax.broadcasted_iota(jnp.int32, (n_pos, 2 * HEAD_DIM), 1) < HEAD_DIM
        for p in pairs:
            cols = slice(p * 2 * HEAD_DIM, (p + 1) * 2 * HEAD_DIM)
            xp = s.hv[:, cols]
            both = []
            for h in (2 * p, 2 * p + 1):
                gap = cum_t[:, h : h + 1] - cum[h : h + 1, :]
                within = jnp.exp(jnp.where(low, gap, -jnp.inf))
                both.append(dot(affinity * within, xp, highest))
            s.scan[:, cols] = jnp.where(pair_lane, both[0], both[1])

    def mixer_group():
        mix_drain(s.st_got, s.m_r, 0)
        mix_drain(s.dec_got, s.m_r, 3)
        run = jnp.zeros((STATE, per), f32)
        run_d = jnp.zeros((8, per), f32)
        for j in range(G):
            s.enter[j, 0:STATE, :] = run
            s.enter[j, STATE : STATE + 8, :] = run_d
            d_j = s.dec_got[j]
            run = s.st_got[j].astype(f32) + jnp.exp(d_j[0:1, :]) * run
            run_d = run_d + d_j
        s.tot_send[0:STATE, :] = run
        s.tot_send[STATE : STATE + 8, :] = run_d

        @pl.loop(1, Z)
        def _(d):
            rc(s.tot_send, s.tot_got.at[z], s.m_s.at[1], s.m_r.at[1], z_peer(d)).start()

        s.tot_got[z] = s.tot_send[...]

    def mixer_enter():
        mix_drain(s.tot_got, s.m_r, 1)
        run = jnp.zeros((STATE, per), f32)
        for j in range(Z):
            new = s.tot_got[j, 0:STATE, :] + jnp.exp(s.tot_got[j, STATE : STATE + 1, :]) * run
            run = jnp.where(j < z, new, run)
        for j in range(G):
            entry = s.enter[j, 0:STATE, :] + jnp.exp(s.enter[j, STATE : STATE + 1, :]) * run
            s.in_send[j] = entry.astype(bf16)
        for d in range(1, G):
            mix_g(s.in_send, s.in_got, 2, d)
        s.in_got[g] = s.in_send[g]

    def mixer_finish():
        mix_drain(s.in_got, s.m_r, 2)
        local.gates.wait()
        rv = s.rv[...]
        square = jnp.zeros((n_pos, 1), f32)
        for j in range(G):
            cols = slice(j * per, (j + 1) * per)
            carried = dot(rv, s.in_got[j].astype(f32), highest) * s.cum_x[:, cols]
            gated = (s.scan[:, cols] + carried) * silu(s.gates[:, cols].astype(f32))
            s.scan[:, cols] = gated
            square = square + jnp.sum(gated * gated, axis=1, keepdims=True)
        scale = lax.rsqrt(square / chans + eps_norm)
        mixed = (s.scan[...] * scale * s.mix_gain[...]).astype(bf16)
        local.mixw.wait()
        mb = n_pos // Y
        for c in range(4):
            cols = slice(c * (width // 4), (c + 1) * (width // 4))
            part = dot(mixed, s.mixw[:, cols]).astype(bf16)
            for j in range(Y):
                s.mix_send[j, :, cols] = part[j * mb : (j + 1) * mb, :]
        s.mix_got[y] = s.mix_send[y]

    def mixer_send():
        @pl.loop(1, Y)
        def _(d):
            rc(
                s.mix_send.at[lax.rem(y + d, Y)], s.mix_got.at[y], s.rs_s.at[0], s.rs_r.at[0], y_peer(d)
            ).start()

    def shared_x(t, d):
        if d == 1:
            sh_y(t).wait_recv()
        sh_x_start(t, d)

    def shared_c():
        for t in range(3):
            sh_x_drain(t, s.shx_r)
            sh_c(t).start()

    def shared_hidden(v, slot):
        return (silu(dot(v, s.full_gate[slot])) * dot(v, s.full_up[slot])).astype(bf16)

    def shared_down(h, q):
        cols = slice(q * (width // 4), (q + 1) * (width // 4))
        return cols, dot(h[0], s.full_down[0, :, cols]) + dot(h[1], s.full_down[1, :, cols])

    def shared_own():
        for t in range(3):
            sh_c(t).wait_recv()
        v = s.normed[...]
        h = (shared_hidden(v, 0), shared_hidden(v, 1))
        for q in range(4):
            cols, new = shared_down(h, q)
            s.sh_own[:, cols] = new

    def shared_pair():
        shared_rows().wait_recv()
        v = s.pair_normed[...]
        h = (shared_hidden(v, 0), shared_hidden(v, 1))
        for q in range(4):
            cols, new = shared_down(h, q)
            s.sh_send[:, cols] = new.astype(bf16)
        shared_return().start()

    def stage_a(c):
        seven(s.recv1, c, s.z_r, 0)
        moved = dot(s.perm[...], s.recv1[:, :, COLS[c]].reshape(slots, -1)).astype(bf16)
        s.perm1[:, :, COLS[c]] = moved.reshape(G, Z * CAP, -1)
        spread_g(s.perm1, s.toks.at[0], c, 0)
        s.toks[0, g, :, COLS[c]] = s.perm1[g, :, COLS[c]]

    def gate_up(t, c):
        v = s.toks[t, :, :, COLS[c]].reshape(slots, -1)
        for acc, refs in ((s.accg, (s.ogate, s.pgu.at[0])), (s.accu, (s.oup, s.pgu.at[1]))):
            for n, ref in enumerate(refs):
                cols = slice(n * ff, (n + 1) * ff)
                new = dot(v, ref[COLS[c], :])
                if c > 0:
                    new = new + acc[t, :, cols]
                acc[t, :, cols] = new

    def stage_b(c):
        seven(s.toks.at[0], c, s.g_r, 0)
        sy(c).start()

    def own_rows(c):
        if c == 0:
            local.gate.wait()
            local.up.wait()
        drain(s.pgu.at[:, COLS[c], :], s.w_r.at[0, c])
        gate_up(0, c)

    def pair_rows(c):
        sy(c).wait_recv()
        gate_up(1, c)

    def hide(t):
        s.hidden[t] = (silu(s.accg[t]) * s.accu[t]).astype(bf16)

    def down(t, c):
        return dot(s.hidden[t, :, 0:ff], s.odown[:, COLS[c]]) + dot(s.hidden[t, :, ff : 2 * ff], s.pdown[:, COLS[c]])

    def back_d(c):
        if c >= CHUNKS:
            return
        if c == 0:
            local.down.wait()
        weight_copy(2, c).wait_recv()
        s.ysend[:, COLS[c]] = down(1, c).astype(bf16)
        ry(c).start()

    def back_e(c):
        mine = down(0, c)
        ry(c).wait_recv()
        total = (mine + s.yrecv[:, COLS[c]].astype(f32)).astype(bf16)
        s.back2[:, :, COLS[c]] = total.reshape(G, Z * CAP, -1)
        spread_g(s.back2, s.got2, c, 1)
        s.got2[g, :, COLS[c]] = s.back2[g, :, COLS[c]]

    def back_f(c):
        seven(s.got2, c, s.g_r, 1)
        moved = dot(s.perm[...], s.got2[:, :, COLS[c]].reshape(slots, -1)).astype(bf16)
        s.back1[:, :, COLS[c]] = moved.reshape(Z, zrows, -1)
        spread_z(s.back1, s.got1, c, 1)
        s.got1[z, :, COLS[c]] = s.back1[z, :, COLS[c]]

    def weights_by_row():
        pick_w = jnp.transpose(s.pick_w[...])
        w_hi = pick_w.astype(bf16)
        s.w_hi[...] = w_hi
        s.w_lo[...] = (pick_w - w_hi.astype(f32)).astype(bf16)

    def early_sends():
        for copy in tail_copies():
            copy.wait_send()
        drain(s.pgu, s.w_s.at[0])
        drain(s.pdown, s.w_s.at[1])
        drain(s.toks.at[0], s.y_s.at[0])
        drain(s.own.at[pl.ds(0, Z - 1)], s.z_s.at[0])
        drain(s.perm1.at[pl.ds(0, G - 1)], s.g_s.at[0])
        for t in range(3):
            sh_y(t).wait_send()
            sh_x_drain(t, s.shx_s)
            sh_c(t).wait_send()
        mix_drain(s.st_got, s.m_s, 0)
        mix_drain(s.dec_got, s.m_s, 3)
        mix_drain(s.tot_got, s.m_s, 1)
        mix_drain(s.in_got, s.m_s, 2)

    extras = {
        1: lambda: mixer_states(),
        2: lambda: mixer_scan(range(0, 2)),
        3: lambda: mixer_scan(range(2, 4)),
        4: lambda: mixer_scan(range(4, 6)),
        5: lambda: mixer_scan(range(6, 8)),
    }
    spare = [(t, d) for t in range(3) for d in range(1, X)]
    mixer_conv()
    local.perm.wait()
    for c in range(CHUNKS):
        stage_a(c)
        if c >= 1:
            stage_b(c - 1)
        if c in extras:
            extras[c]()
        if 1 <= c < G:
            mix_g(s.st_send, s.st_got, 0, c)
            mix_g(s.dec_send, s.dec_got, 3, c)
        if c >= 2:
            for t, d in spare[2 * (c - 2) : 2 * (c - 1)]:
                shared_x(t, d)
            own_rows(c - 2)
        if c >= 4:
            pair_rows(c - 4)
    stage_b(CHUNKS - 1)
    mixer_group()
    shared_c()
    for c in range(CHUNKS - 4, CHUNKS):
        if c >= CHUNKS - 2:
            own_rows(c)
        pair_rows(c)
    hide(1)
    back_d(0)
    back_d(1)
    hide(0)
    back_d(2)
    after = {
        0: lambda: mixer_enter(),
        2: lambda: mixer_finish(),
        3: lambda: shared_own(),
        4: lambda: weights_by_row(),
        5: lambda: shared_pair(),
        7: lambda: early_sends(),
        CHUNKS: lambda: mixer_send(),
    }
    for c in range(CHUNKS + 1):
        back_d(c + 3)
        if c < CHUNKS:
            back_e(c)
        if c >= 1:
            back_f(c - 1)
        if c in after:
            after[c]()

    def moe_copy(c):
        return pltpu.make_async_copy(s.moe_res.at[:, COLS[c]], moe_out.at[:, COLS[c]], s.out.at[0])

    def mix_sum():
        drain(s.mix_got.at[pl.ds(0, Y - 1)], s.rs_r.at[0])
        mix = jnp.zeros(s.mix_res.shape, f32)
        for j in range(Y):
            mix = mix + s.mix_got[j].astype(f32)
        s.mix_res[...] = mix.astype(bf16)

    mix_copy = pltpu.make_async_copy(s.mix_res, mix_out, s.out.at[1])
    shared_rows().wait_send()
    shared_return().wait()
    drain(s.ysend, s.y_s.at[1])
    for c in range(CHUNKS):
        if c == CHUNKS - 1:
            drain(s.back2.at[pl.ds(0, G - 1)], s.g_s.at[1])
            drain(s.back1.at[pl.ds(0, Z - 1)], s.z_s.at[1])
            mix_sum()
            mix_copy.start()
            drain(s.mix_send.at[pl.ds(0, Y - 1)], s.rs_s.at[0])
        seven(s.got1, c, s.z_r, 1)
        v = s.got1[:, :, COLS[c]].reshape(slots, -1)
        shared = s.sh_own[:, COLS[c]] + s.sh_recv[:, COLS[c]].astype(f32)
        total = dot(s.w_hi[...], v) + dot(s.w_lo[...], v) + shared
        s.moe_res[:, COLS[c]] = total.astype(bf16)
        moe_copy(c).start()
    mix_copy.wait()
    drain(s.moe_res, s.out.at[0])


def local(
    heads, write, read, gates, step, extra, decay, head_taps, write_taps, read_taps, mix_gain,
    mix_weight, rows, row_gain, routes, scores, gate_w, up_w, down_w, sh_gate, sh_up, sh_down,
):
    n_pos, chans = heads.shape
    tok, width = rows.shape
    ff = gate_w.shape[2]
    sff = sh_gate.shape[1]
    slots = Z * G * CAP
    per = chans // G
    order = np.arange(slots).reshape(G, Z, CAP).transpose(1, 0, 2).reshape(-1)
    perm = jnp.asarray(np.eye(slots, dtype=np.float32)[order], bf16)
    dma = pltpu.SemaphoreType.DMA
    blocks = (Z, G * CAP, width)
    scratch = dict(
        tail_heads=((16, chans), bf16),
        tail_write=((16, STATE), bf16),
        tail_read=((16, STATE), bf16),
        ogate=((width, ff), bf16),
        oup=((width, ff), bf16),
        odown=((ff, width), bf16),
        pgu=((2, width, ff), bf16),
        pdown=((ff, width), bf16),
        mixw=((chans, width), bf16),
        full_gate=((2, width, sff), bf16),
        full_up=((2, width, sff), bf16),
        full_down=((2, sff, width), bf16),
        pair_normed=((tok, width), bf16),
        sh_send=((tok, width), bf16),
        sh_recv=((tok, width), bf16),
        gates=((n_pos, chans), bf16),
        normed=((tok, width), bf16),
        sh_own=((tok, width), f32),
        pick_w=((slots, tok), f32),
        w_hi=((tok, slots), bf16),
        w_lo=((tok, slots), bf16),
        own=(blocks, bf16),
        recv1=(blocks, bf16),
        perm1=(blocks, bf16),
        toks=((2, *blocks), bf16),
        accg=((2, slots, 2 * ff), f32),
        accu=((2, slots, 2 * ff), f32),
        hidden=((2, slots, 2 * ff), bf16),
        ysend=((slots, width), bf16),
        yrecv=((slots, width), bf16),
        back2=(blocks, bf16),
        got2=(blocks, bf16),
        back1=(blocks, bf16),
        got1=(blocks, bf16),
        ext=((n_pos + 16, chans + 2 * STATE), f32),
        hv=((n_pos, chans), f32),
        wv=((n_pos, STATE), f32),
        rv=((n_pos, STATE), f32),
        cum=((step.shape[0], n_pos), f32),
        affinity=((n_pos, n_pos), f32),
        cum_x=((n_pos, chans), f32),
        scan=((n_pos, chans), f32),
        st_send=((G, STATE, per), bf16),
        st_got=((G, STATE, per), bf16),
        dec_send=((G, 8, per), f32),
        dec_got=((G, 8, per), f32),
        enter=((G, STATE + 8, per), f32),
        tot_send=((STATE + 8, per), f32),
        tot_got=((Z, STATE + 8, per), f32),
        in_send=((G, STATE, per), bf16),
        in_got=((G, STATE, per), bf16),
        mix_send=((Y, n_pos // Y, width), bf16),
        mix_got=((Y, n_pos // Y, width), bf16),
        mix_res=((n_pos // Y, width), bf16),
        moe_res=((tok, width), bf16),
    )
    sems = dict(
        tail_s=(3,), tail_r=(3,), w_s=(2,), w_r=(2, CHUNKS), shy_s=(3,), shy_r=(3,), shx_s=(3,), shx_r=(3,), shc_s=(3,),
        shc_r=(3,), st_s=(2,), st_r=(2,), z_s=(2,), z_r=(2, CHUNKS), g_s=(2,), g_r=(2, CHUNKS), y_s=(2,),
        y_r=(2, CHUNKS), m_s=(4,), m_r=(4,), rs_s=(1,), rs_r=(1,), loc=(23,), out=(2,),
    )
    inputs = dict(
        gates=gates, mix_weight=mix_weight, gate_w=gate_w, up_w=up_w, down_w=down_w, sh_gate=sh_gate, sh_up=sh_up,
        sh_down=sh_down,
    )
    copied = dict(
        heads=heads, write=write, read=read, step=step, extra=extra, decay=decay.reshape(1, -1), head_taps=head_taps,
        write_taps=write_taps, read_taps=read_taps, mix_gain=mix_gain.reshape(1, -1), rows=rows,
        row_gain=row_gain.reshape(1, -1), routes=routes.T, scores=scores.T, perm=perm,
    )
    scratch.update((n, (v.shape, v.dtype)) for n, v in copied.items())
    inputs.update(copied)
    names = list(scratch) + list(sems)
    shapes = [pltpu.VMEM(*v) for v in scratch.values()] + [dma(v) for v in sems.values()]
    hbm = pl.BlockSpec(memory_space=pl.ANY)
    return pl.pallas_call(
        make_kernel(list(inputs), names),
        name="mixer_moe",
        out_shape=(
            jax.ShapeDtypeStruct((n_pos // Y, width), bf16),
            jax.ShapeDtypeStruct((tok, width), bf16),
        ),
        in_specs=[hbm] * len(inputs),
        out_specs=(hbm, hbm),
        scratch_shapes=shapes,
        compiler_params=pltpu.CompilerParams(
            collective_id=0, has_side_effects=True, vmem_limit_bytes=67043328
        ),
    )(*inputs.values())


def solution(mesh):
    split = Mesh(mesh.devices.reshape(8, 4, 2, mesh.shape["tp"]), ("ep_0", "ep_1", "ep_2", "tp"))
    placed = (
        P(EP, "tp"),
        P(EP, "tp"),
        P(EP, "tp"),
        P(EP, "tp"),
        P("tp", EP),
        P("tp", EP),
        P("tp"),
        P(None, "tp"),
        P(None, "tp"),
        P(None, "tp"),
        P("tp"),
        P("tp", None),
        P(EP_TP, None),
        P(),
        P(EP_TP, None),
        P(EP_TP, None),
        P(EP, None, "tp"),
        P(EP, None, "tp"),
        P(EP, "tp", None),
        P(None, "tp"),
        P(None, "tp"),
        P("tp", None),
    )
    return jax.shard_map(
        local,
        mesh=split,
        in_specs=placed,
        out_specs=(P(EP_TP, None), P(EP_TP, None)),
        check_vma=False,
    )
```

time: 433 us -> 120 us (0.28)
  waiting for transfers between devices: 157 us -> 0 us
  Pallas kernels: 0 us -> 115 us
  blocking collectives: 99 us -> 0 us
  local copies, waits for them, and re-layouts: 56.7 us -> 3.45 us
  matrix products: 42.5 us -> 0 us
  other arithmetic: 32.3 us -> 0 us
  starting transfers between devices: 26.7 us -> 0 us
  between operations: 14.9 us -> 0.65 us
    pallas_call x0 -> x1, Pallas kernels: none -> 115 us  [local(): pl.pallas_call(make_kernel(list(inputs), names), name='mixer_moe', out_sh...]
    all_gather x5 -> x0, waiting for transfers between devices: 85.8 us -> none  [the longest x1 53.5 us: local(): arrived = lax.all_gather(own_arrived[None], 'tp', axis=0, tiled=True)]
    all_to_all x3 -> x0, waiting for transfers between devices: 70.2 us -> none  [the longest x1 40.2 us: local(): lax.all_to_all(summed.reshape(ep_count * local_experts, capacity, model_w...]
    all_to_all x1 -> x0, blocking collectives: 59.4 us -> none  [local(): lax.all_to_all(own_out, EP, split_axis=0, concat_axis=0, tiled=True)]
    dot_general x11 -> x0, matrix products: 42.5 us -> none  [the longest x1 12.6 us: local(): jnp.einsum('osecf,efd->osecd', hidden, routed_down_weight, preferred_elem...]
    all_gather x5 -> x0, blocking collectives: 39.6 us -> none  [the longest x3 24.5 us: entering_2(): pieces = jax.tree.map(lambda part: lax.all_gather(part, axis), running)]
    all_to_all x3 -> x0, starting transfers between devices: 22 us -> none  [the longest x1 12.7 us: local(): lax.all_to_all(summed.reshape(ep_count * local_experts, capacity, model_w...]
    convert_element_type x2 -> x0, local copies, waits for them, and re-layouts: 22 us -> none  [the longest x1 18.3 us: local(): partial_value = jnp.einsum('osecf,efd->osecd', hidden, routed_down_weight...]
  transfers between devices with their start and end apart: 9 -> 0, of which waited for: 6 -> 0; matrix products, arithmetic and copies ran while one was open for 25% -> 0% of each run, Pallas kernels for 0% -> 0%
where the time goes in v1:
time: 120 us; the launch traced here: 119 us
  Pallas kernels  115 us (96%)
  local copies, waits for them, and re-layouts  3.45 us (3%)
    pallas_call x1, Pallas kernels, local(): pl.pallas_call(make_kernel(list(inputs), names), name='mixer_moe', out_sh...  115 us
    unnamed x2, local copies, waits for them, and re-layouts  3.45 us

profile of v1, /device:TPU:1, one launch (start us, length us, event | category | flops | bytes accessed | tf_op | source)
XLA Modules:
  0.0 119.5 jit_solution(15275974589657418254)
XLA Ops:
  0.6 115.4 %mixer_moe.1 = (bf16[32,2048]{1,0:T(8,128)(2,1)}, bf16[128,2048]{1,0:T(8,128)(2,1)}) custom-call(bf16[128,1024]{1,0:T(8,128)(2,1)} %refs_0_.1, bf16[1024,2048]{1,0:T(8,128)(2,1)} %refs_1_.1, bf16[1,2048,256]{2,1,0:T(8,128)(2,1)} %refs_2_.1, bf16[1,2048,256]{2,1,0:T(8,128)(2,1)} %refs_3_.1, bf16[1,256,2048]{2,1,0:T(8,128)(2,1)} %refs_4_.1, ...), custom_call_target="tpu_custom_call" | custom-call | tf_op jit(solution)/shard_map/mixer_moe/pallas_call | solution.py:724
  116.0 1.6 %copy.27 = bf16[32,2048]{1,0:T(8,128)(2,1)} copy(bf16[32,2048]{1,0:T(8,128)(2,1)} %get-tuple-element.4) | data formatting | bytes 262144
  117.6 1.9 %copy.28 = bf16[128,2048]{1,0:T(8,128)(2,1)} copy(bf16[128,2048]{1,0:T(8,128)(2,1)} %get-tuple-element.5) | data formatting | bytes 1048576

commit v2 on v1

--- a/solution.py
+++ b/solution.py
@@ -10,7 +10,7 @@
 HEAD_DIM = 64
 STATE = 128
 CAP = 6
-SIZES = (128, 256, 256, 256, 256, 256, 256, 256, 128)
+SIZES = (128, 256, 256, 256, 256, 256, 256, 128, 128, 128)
 CHUNKS = len(SIZES)
 COLS = tuple(slice(sum(SIZES[:c]), sum(SIZES[: c + 1])) for c in range(CHUNKS))
 Z, X, G, Y = 8, 4, 8, 4
@@ -552,7 +552,6 @@
         4: lambda: mixer_scan(range(4, 6)),
         5: lambda: mixer_scan(range(6, 8)),
     }
-    spare = [(t, d) for t in range(3) for d in range(1, X)]
     mixer_conv()
     local.perm.wait()
     for c in range(CHUNKS):
@@ -565,14 +564,14 @@
             mix_g(s.st_send, s.st_got, 0, c)
             mix_g(s.dec_send, s.dec_got, 3, c)
         if c >= 2:
-            for t, d in spare[2 * (c - 2) : 2 * (c - 1)]:
-                shared_x(t, d)
             own_rows(c - 2)
         if c >= 4:
             pair_rows(c - 4)
     stage_b(CHUNKS - 1)
     mixer_group()
-    shared_c()
+    for t in range(3):
+        for d in range(1, X):
+            shared_x(t, d)
     for c in range(CHUNKS - 4, CHUNKS):
         if c >= CHUNKS - 2:
             own_rows(c)
@@ -584,6 +583,7 @@
     back_d(2)
     after = {
         0: lambda: mixer_enter(),
+        1: lambda: shared_c(),
         2: lambda: mixer_finish(),
         3: lambda: shared_own(),
         4: lambda: weights_by_row(),
@@ -629,6 +629,19 @@
         moe_copy(c).start()
     mix_copy.wait()
     drain(s.moe_res, s.out.at[0])
+
+
+def settle(mix_in, moe_in, mix_out, moe_out, mix, moe, sems):
+    pairs = ((mix_in, mix, mix_out), (moe_in, moe, moe_out))
+    into = [pltpu.make_async_copy(a, v, sems.at[k]) for k, (a, v, _) in enumerate(pairs)]
+    out = [pltpu.make_async_copy(v, b, sems.at[k + 2]) for k, (_, v, b) in enumerate(pairs)]
+    for copy in into:
+        copy.start()
+    for arrived, copy in zip(into, out):
+        arrived.wait()
+        copy.start()
+    for copy in out:
+        copy.wait()
 
 
 def local(
@@ -721,13 +734,14 @@
     names = list(scratch) + list(sems)
     shapes = [pltpu.VMEM(*v) for v in scratch.values()] + [dma(v) for v in sems.values()]
     hbm = pl.BlockSpec(memory_space=pl.ANY)
-    return pl.pallas_call(
+    outs = (
+        jax.ShapeDtypeStruct((n_pos // Y, width), bf16),
+        jax.ShapeDtypeStruct((tok, width), bf16),
+    )
+    results = pl.pallas_call(
         make_kernel(list(inputs), names),
         name="mixer_moe",
-        out_shape=(
-            jax.ShapeDtypeStruct((n_pos // Y, width), bf16),
-            jax.ShapeDtypeStruct((tok, width), bf16),
-        ),
+        out_shape=outs,
         in_specs=[hbm] * len(inputs),
         out_specs=(hbm, hbm),
         scratch_shapes=shapes,
@@ -735,6 +749,14 @@
             collective_id=0, has_side_effects=True, vmem_limit_bytes=67043328
         ),
     )(*inputs.values())
+    return pl.pallas_call(
+        settle,
+        name="settle",
+        out_shape=outs,
+        in_specs=[hbm] * 2,
+        out_specs=(hbm, hbm),
+        scratch_shapes=[pltpu.VMEM(v.shape, v.dtype) for v in outs] + [dma((4,))],
+    )(*results)
 
 
 def solution(mesh):

time: 120 us -> 117 us (0.975)
  local copies, waits for them, and re-layouts: 3.45 us -> 0 us
    unnamed x2 -> x0, local copies, waits for them, and re-layouts: 3.45 us -> none
    pallas_call x0 -> x1, Pallas kernels: none -> 1.94 us  [local(): pl.pallas_call(settle, name='settle', out_shape=outs, in_specs=[hbm] * 2,...]
    pallas_call x1, Pallas kernels: 115 us -> 114 us  [local(): pl.pallas_call(make_kernel(list(inputs), names), name='mixer_moe', out_sh...]
where the time goes in v2:
time: 117 us
  Pallas kernels  116 us (99%)
    pallas_call x1, Pallas kernels, local(): pl.pallas_call(make_kernel(list(inputs), names), name='mixer_moe', out_sh...  114 us

profile of v2, /device:TPU:1, one launch (start us, length us, event | category | flops | bytes accessed | tf_op | source)
XLA Modules:
  0.0 116.5 jit_solution(3621530078199352016)
XLA Ops:
  0.6 113.8 %mixer_moe.1 = (bf16[32,2048]{1,0:T(8,128)(2,1)}, bf16[128,2048]{1,0:T(8,128)(2,1)}) custom-call(bf16[128,1024]{1,0:T(8,128)(2,1)} %refs_0_.1, bf16[1024,2048]{1,0:T(8,128)(2,1)} %refs_1_.1, bf16[1,2048,256]{2,1,0:T(8,128)(2,1)} %refs_2_.1, bf16[1,2048,256]{2,1,0:T(8,128)(2,1)} %refs_3_.1, bf16[1,256,2048]{2,1,0:T(8,128)(2,1)} %refs_4_.1, ...), custom_call_target="tpu_custom_call" | custom-call | tf_op jit(solution)/shard_map/mixer_moe/pallas_call | solution.py:741
  114.4 1.9 %settle.1 = (bf16[32,2048]{1,0:T(8,128)(2,1)}, bf16[128,2048]{1,0:T(8,128)(2,1)}) custom-call(bf16[32,2048]{1,0:T(8,128)(2,1)} %get-tuple-element.4.mix_in, bf16[128,2048]{1,0:T(8,128)(2,1)} %get-tuple-element.5.moe_in), custom_call_target="tpu_custom_call" | custom-call | tf_op jit(solution)/shard_map/settle/pallas_call | solution.py:752

commit v3 on v2

--- a/solution.py
+++ b/solution.py
@@ -10,7 +10,7 @@
 HEAD_DIM = 64
 STATE = 128
 CAP = 6
-SIZES = (128, 256, 256, 256, 256, 256, 256, 128, 128, 128)
+SIZES = (128, 256, 256, 256, 256, 256, 256, 256, 128)
 CHUNKS = len(SIZES)
 COLS = tuple(slice(sum(SIZES[:c]), sum(SIZES[: c + 1])) for c in range(CHUNKS))
 Z, X, G, Y = 8, 4, 8, 4
@@ -104,18 +104,6 @@
 
     def greet(dev):
         pl.semaphore_signal(barrier, inc=1, device_id=dev, device_id_type=MESH)
-
-    @pl.loop(1, Z)
-    def _(d):
-        greet(z_peer(d))
-        greet(g_peer(d))
-
-    @pl.loop(1, Y)
-    def _(d):
-        greet(y_peer(d))
-
-    greet(ep_peer(1))
-    greet(ep_peer(-1))
 
     def tail_copies():
         last = pl.ds(n_pos - 16, 16)
@@ -229,11 +217,22 @@
         down=fetched(i.down_w.at[0], s.odown),
         mixw=fetched(i.mix_weight, s.mixw),
     )
-    for copy in small_in + list(local.values()):
+    for copy in small_in[:4]:
         copy.start()
+    @pl.loop(1, Z)
+    def _(d):
+        greet(z_peer(d))
+        greet(g_peer(d))
+
+    @pl.loop(1, Y)
+    def _(d):
+        greet(y_peer(d))
+
+    greet(ep_peer(1))
+    greet(ep_peer(-1))
     local = Names(local.keys(), local.values())
-    for copy in small_in[:4]:
-        copy.wait()
+    small_in[0].wait()
+    small_in[1].wait()
     route = s.routes[...]
     score = s.scores[...].astype(f32)
     weight = score / jnp.sum(score, axis=0, keepdims=True) * route_scale
@@ -253,6 +252,10 @@
         pick_w = pick_w + jnp.where(here, weight[k : k + 1, :], 0.0)
     s.pick_w[...] = pick_w
     pick = pick.astype(bf16)
+    for copy in small_in[4:] + list(local.__dict__.values()):
+        copy.start()
+    small_in[2].wait()
+    small_in[3].wait()
     rows = s.rows[...].astype(f32)
     normed = (
         rows * lax.rsqrt(jnp.mean(rows * rows, axis=1, keepdims=True) + eps_norm) * s.row_gain[...]
@@ -563,19 +566,19 @@
         if 1 <= c < G:
             mix_g(s.st_send, s.st_got, 0, c)
             mix_g(s.dec_send, s.dec_got, 3, c)
-        if c >= 2:
-            own_rows(c - 2)
         if c >= 4:
-            pair_rows(c - 4)
+            own_rows(c - 4)
+        if c >= 5:
+            pair_rows(c - 5)
     stage_b(CHUNKS - 1)
     mixer_group()
     for t in range(3):
         for d in range(1, X):
             shared_x(t, d)
     for c in range(CHUNKS - 4, CHUNKS):
-        if c >= CHUNKS - 2:
-            own_rows(c)
-        pair_rows(c)
+        own_rows(c)
+        pair_rows(c - 1)
+    pair_rows(CHUNKS - 1)
     hide(1)
     back_d(0)
     back_d(1)

time: 117 us -> 116 us (level)
  no operation moved by 1% of the time
where the time goes in v3:
time: 116 us
  Pallas kernels  115 us (99%)
    pallas_call x1, Pallas kernels, local(): pl.pallas_call(make_kernel(list(inputs), names), name='mixer_moe', out_sh...  114 us

profile of v3, /device:TPU:1, one launch (start us, length us, event | category | flops | bytes accessed | tf_op | source)
XLA Modules:
  0.0 116.3 jit_solution(5918081285310317657)
XLA Ops:
  0.6 113.5 %mixer_moe.1 = (bf16[32,2048]{1,0:T(8,128)(2,1)}, bf16[128,2048]{1,0:T(8,128)(2,1)}) custom-call(bf16[128,1024]{1,0:T(8,128)(2,1)} %refs_0_.1, bf16[1024,2048]{1,0:T(8,128)(2,1)} %refs_1_.1, bf16[1,2048,256]{2,1,0:T(8,128)(2,1)} %refs_2_.1, bf16[1,2048,256]{2,1,0:T(8,128)(2,1)} %refs_3_.1, bf16[1,256,2048]{2,1,0:T(8,128)(2,1)} %refs_4_.1, ...), custom_call_target="tpu_custom_call" | custom-call | tf_op jit(solution)/shard_map/mixer_moe/pallas_call | solution.py:744
  114.2 1.9 %settle.1 = (bf16[32,2048]{1,0:T(8,128)(2,1)}, bf16[128,2048]{1,0:T(8,128)(2,1)}) custom-call(bf16[32,2048]{1,0:T(8,128)(2,1)} %get-tuple-element.4.mix_in, bf16[128,2048]{1,0:T(8,128)(2,1)} %get-tuple-element.5.moe_in), custom_call_target="tpu_custom_call" | custom-call | tf_op jit(solution)/shard_map/settle/pallas_call | solution.py:755
